TPU v7x, 32 devices: a whole 2x2x4 slice. The times are simulated.
32 devices in a mesh: sp: 4 (over z), dp: 8 (over y, x, core).
Axes of the slice: x: 2, y: 2, z: 4, core: 2. Of those that a mesh axis runs over, the one named last changes fastest.
Arguments:
- queries: bfloat16 [8, 768, 6144], P('dp', None, 'sp'), may hold values from -64 to 64
- out_grad: bfloat16 [8, 768, 4096], P('dp', None, 'sp'), may hold values from -6 to 6
- latent: bfloat16 [8, 768, 512], P('dp'), may hold values from -6 to 6
- rope_key: bfloat16 [8, 768, 64], P('dp'), may hold values from -6 to 6
- kv_gain: float32 [512], replicated, may hold values from 0.1 to 1.9
- key_up: bfloat16 [512, 4096], P('dp', 'sp'), may hold values from -0.25 to 0.25
- value_up: bfloat16 [512, 4096], P('dp', 'sp'), may hold values from -0.25 to 0.25
Outputs:
- query_grad: bfloat16 [8, 768, 6144], P('dp', None, 'sp')
- latent_grad: bfloat16 [8, 768, 512], P('dp')
- rope_key_grad: bfloat16 [8, 768, 64], P('dp')
- key_up_grad: float32 [512, 4096], P('dp', 'sp')
- value_up_grad: float32 [512, 4096], P('dp', 'sp')
All inputs are finite; a program needn't handle non-finite values.
Results may differ from a plain program's by a relative error of at most 0.019.
The roundings to bfloat16 on the way count: a program that leaves them out, or rounds other values in their place, can miss the bound.
Values may be sent and summed in bfloat16 or wider, within the bound.
A program may use at most 64 MiB of HBM per device.

v0:
```python
import jax
import jax.numpy as jnp
from jax import lax
from jax.sharding import PartitionSpec as P

NOPE_DIM = 128
ROPE_DIM = 64
VALUE_DIM = 128
norm_eps = 1e-06
rope_theta = 10000.0


def rope_tables(length, width):
    half_width = width // 2
    frequency = rope_theta ** (-(jnp.arange(half_width, dtype=jnp.float32) * 2.0 / width))
    position = jnp.arange(length, dtype=jnp.int32).astype(jnp.float32)
    angles = position[:, None] * frequency[None, :]
    return (jnp.cos(angles), jnp.sin(angles))


def rotate(tensor, cosine, sine_table):
    half_width = tensor.shape[-1] // 2
    first_half = tensor[..., :half_width]
    second = tensor[..., half_width:]
    return jnp.concatenate(
        [first_half * cosine - second * sine_table, second * cosine + first_half * sine_table],
        axis=-1,
    )


def unrotate(upstream, cosine, sine_table):
    half_width = upstream.shape[-1] // 2
    first_half = upstream[..., :half_width]
    second = upstream[..., half_width:]
    return jnp.concatenate(
        [first_half * cosine + second * sine_table, second * cosine - first_half * sine_table],
        axis=-1,
    )


def head_backward(query_used, key_used, head_value, head_grad, score_scale):
    length = query_used.shape[0]
    scores = jnp.dot(query_used, key_used.T, preferred_element_type=jnp.float32) * score_scale
    causal = lax.broadcasted_iota(jnp.int32, (length, length), 0) >= lax.broadcasted_iota(
        jnp.int32, (length, length), 1
    )
    scores = jnp.where(causal, scores, -jnp.inf)
    row_top = jnp.max(scores, axis=1, keepdims=True)
    weights = jnp.exp(scores - row_top)
    probs = weights / jnp.sum(weights, axis=1, keepdims=True)
    probs_low = probs.astype(jnp.bfloat16)
    value_grad = jnp.dot(probs_low.T, head_grad, preferred_element_type=jnp.float32).astype(
        jnp.bfloat16
    )
    prob_grad = jnp.dot(head_grad, head_value.T, preferred_element_type=jnp.float32)
    center = jnp.sum(probs * prob_grad, axis=1, keepdims=True)
    score_grad = (probs * (prob_grad - center) * score_scale).astype(jnp.bfloat16)
    query_grad = jnp.dot(score_grad, key_used, preferred_element_type=jnp.float32)
    key_grad = jnp.dot(score_grad.T, query_used, preferred_element_type=jnp.float32)
    return (query_grad, key_grad, value_grad)


def attend(queries, head_grads, keys, values, key_rot, cosine, sine_table):
    length = queries.shape[0]
    head_count = head_grads.shape[1] // VALUE_DIM
    qk_width = NOPE_DIM + ROPE_DIM
    query_heads = queries.reshape(length, head_count, qk_width)
    rotated = rotate(
        query_heads[:, :, NOPE_DIM:].astype(jnp.float32), cosine[:, None, :], sine_table[:, None, :]
    ).astype(jnp.bfloat16)
    query_used = jnp.concatenate([query_heads[:, :, :NOPE_DIM], rotated], axis=-1).transpose(
        1, 0, 2
    )
    key_heads = keys.reshape(length, head_count, NOPE_DIM).transpose(1, 0, 2)
    key_used = jnp.concatenate(
        [key_heads, jnp.broadcast_to(key_rot[None], (head_count, length, ROPE_DIM))], axis=-1
    )
    value_heads = values.reshape(length, head_count, VALUE_DIM).transpose(1, 0, 2)
    grad_heads = head_grads.reshape(length, head_count, VALUE_DIM).transpose(1, 0, 2)
    score_scale = qk_width ** (-0.5)
    query_part, key_part, value_part = lax.map(
        lambda items: head_backward(items[0], items[1], items[2], items[3], score_scale),
        (query_used, key_used, value_heads, grad_heads),
    )
    query_rot_grad = unrotate(query_part[:, :, NOPE_DIM:], cosine[None], sine_table[None])
    query_grad = jnp.concatenate([query_part[:, :, :NOPE_DIM], query_rot_grad], axis=-1).astype(
        jnp.bfloat16
    )
    query_grad = query_grad.transpose(1, 0, 2).reshape(length, head_count * qk_width)
    key_plain_grad = (
        key_part[:, :, :NOPE_DIM]
        .astype(jnp.bfloat16)
        .transpose(1, 0, 2)
        .reshape(length, head_count * NOPE_DIM)
    )
    key_rot_grad = jnp.sum(key_part[:, :, NOPE_DIM:], axis=0)
    value_grad = value_part.transpose(1, 0, 2).reshape(length, head_count * VALUE_DIM)
    return (query_grad, key_plain_grad, key_rot_grad, value_grad)


def finish(comp_total, rot_total, raw_latent, inverse, kv_gain, cosine, sine_table):
    mixed = comp_total * kv_gain
    spread = jnp.mean(raw_latent * mixed, axis=-1, keepdims=True)
    latent_grad = (inverse * mixed - raw_latent * inverse**3 * spread).astype(jnp.bfloat16)
    rope_grad = unrotate(rot_total, cosine, sine_table).astype(jnp.bfloat16)
    return (latent_grad, rope_grad)


def shards(queries, out_grad, latent, rope_key, kv_gain, key_up, value_up):
    key_whole, value_whole = (
        lax.all_gather(key_up, "dp", axis=0, tiled=True),
        lax.all_gather(value_up, "dp", axis=0, tiled=True),
    )
    batch_count, seq_count, latent_width = latent.shape
    raw_latent = latent.astype(jnp.float32)
    inverse = lax.rsqrt(jnp.mean(raw_latent * raw_latent, axis=-1, keepdims=True) + norm_eps)
    compressed = (raw_latent * inverse * kv_gain).astype(jnp.bfloat16)
    cosine, sine_table = rope_tables(seq_count, ROPE_DIM)
    key_rot = rotate(rope_key.astype(jnp.float32), cosine, sine_table).astype(jnp.bfloat16)
    flat_comp = compressed.reshape(batch_count * seq_count, latent_width)
    keys = jnp.dot(flat_comp, key_whole, preferred_element_type=jnp.float32).astype(jnp.bfloat16)
    values = jnp.dot(flat_comp, value_whole, preferred_element_type=jnp.float32).astype(
        jnp.bfloat16
    )
    keys = keys.reshape(batch_count, seq_count, key_whole.shape[1])
    values = values.reshape(batch_count, seq_count, value_whole.shape[1])

    def per_sequence(items):
        query_grad, key_plain_grad, key_rot_grad, value_grad = attend(
            items[0], items[1], items[2], items[3], items[4], cosine, sine_table
        )
        comp_part = jnp.dot(
            key_plain_grad, key_whole.T, preferred_element_type=jnp.float32
        ) + jnp.dot(value_grad, value_whole.T, preferred_element_type=jnp.float32)
        return (query_grad, key_plain_grad, value_grad, comp_part, key_rot_grad)

    query_grad, key_plain_grad, value_grad, comp_part, rot_part = lax.map(
        per_sequence, (queries, out_grad, keys, values, key_rot)
    )
    grad_pair = jnp.concatenate([key_plain_grad, value_grad], axis=-1).reshape(
        batch_count * seq_count, -1
    )
    grad_scale = float(lax.axis_size("dp") * batch_count * seq_count) ** (-0.5)
    comp_total = lax.psum(comp_part.astype(jnp.bfloat16), "sp").astype(jnp.float32)
    rot_total = lax.psum(rot_part.astype(jnp.bfloat16), "sp").astype(jnp.float32)
    latent_grad, rope_grad = finish(
        comp_total, rot_total, raw_latent, inverse, kv_gain, cosine, sine_table
    )
    product = lax.dot_general(
        flat_comp, grad_pair, (((0,), (0,)), ((), ())), preferred_element_type=jnp.float32
    )
    combined = lax.psum_scatter(product * grad_scale, "dp", scatter_dimension=0, tiled=True)
    split_at = key_up.shape[1]
    return (query_grad, latent_grad, rope_grad, combined[:, :split_at], combined[:, split_at:])


def solution(mesh):
    return jax.shard_map(
        shards,
        mesh=mesh,
        in_specs=(
            P("dp", None, "sp"),
            P("dp", None, "sp"),
            P("dp", None, None),
            P("dp", None, None),
            P(),
            P("dp", "sp"),
            P("dp", "sp"),
        ),
        out_specs=(
            P("dp", None, "sp"),
            P("dp", None, None),
            P("dp", None, None),
            P("dp", "sp"),
            P("dp", "sp"),
        ),
        check_vma=False,
    )
```

profile of v0, /device:TPU:0, one launch (start us, length us, event | category | flops | bytes accessed | tf_op | source)
XLA Modules:
  0.0 271.9 jit_solution(8573621979364724312)
XLA Ops:
  10.3 2.6 copy.21
  12.9 2.8 %copy.18 = bf16[1,768,1536]{1,2,0:T(8,128)(2,1)S(1)} copy(bf16[1,768,1536]{2,1,0:T(8,128)(2,1)} %param.9) | data formatting | bytes 4718592 | tf_op args[0]
  19.8 16.2 %all-gather.5.cloned.1.call-done = bf16[512,1024]{1,0:T(8,128)(2,1)} async-done(((bf16[64,1024]{1,0:T(8,128)(2,1)}), bf16[512,1024]{1,0:T(8,128)(2,1)}) %all-gather.5.cloned.1.call-update) | async-done | bytes 1048592 | tf_op jit(solution)/shard_map/all_gather | solution.py:112
  36.0 2.3 fusion.43
  39.7 21.6 %all-gather.3.cloned.1.call-done = bf16[512,1024]{1,0:T(8,128)(2,1)} async-done(((bf16[64,1024]{1,0:T(8,128)(2,1)}), bf16[512,1024]{1,0:T(8,128)(2,1)}) %all-gather.3.cloned.1.call-update) | async-done | bytes 1048592 | tf_op jit(solution)/shard_map/all_gather | solution.py:111
  61.3 2.3 fusion.42
  64.0 2.3 pad_maximum_fusion
  66.4 88.8 %while.19 = (s32[]{:T(128)}, f32[8,768,192]{1,2,0:T(8,128)}, f32[8,768,192]{1,2,0:T(8,128)}, bf16[8,768,128]{1,2,0:T(8,128)(2,1)}, bf16[8,768,192]{1,2,0:T(8,128...) while((s32[]{:T(128)}, f32[8,768,192]{1,2,0:T(8,128)}, ...), condition=%wide.region_5.6_spmd, body=%wide.region_1.5_spmd.sunk | while | flops 992769792 | bytes 24220780 | solution.py:81
  72.8 2.3 fusion.99
  75.2 2.3 fusion.98
  83.9 2.4 fusion.99
  86.3 2.2 fusion.98
  95.0 2.3 fusion.99
  97.3 2.3 fusion.98
  106.1 2.4 fusion.99
  108.5 2.3 fusion.98
  117.2 2.3 fusion.99
  119.5 2.3 fusion.98
  128.3 2.4 fusion.99
  130.7 2.2 fusion.98
  139.4 2.4 fusion.99
  141.8 2.3 fusion.98
  150.5 2.4 fusion.99
  152.9 2.3 fusion.98
  155.1 2.2 slice_reduce_fusion
  157.4 2.1 slice.115
  161.1 1.9 fusion.44
  163.3 5.5 %convolution_multiply_fusion = f32[512,2048]{1,0:T(8,128)} fusion(bf16[1,768,1024]{1,2,0:T(8,128)(2,1)} %bitcast.133, bf16[1,768,1024]{1,2,0:T(8,128)(2,1)S(1)} %bitcast.131, bf16[1,768,512]{2,1,0:T(8,128)(2,1)S(1)} %copy-done, f32[512]{0:T(512)S(1)} %copy-done.9, f32[768]{0:T(1024)S(1)} %copy-done.7), kind=kOutput, calls=%fused_computation.36 | convolution fusion | flops 1619525632 | bytes 8131584 | tf_op jit(solution)/shard_map/dot_general | solution.py:149
  168.9 2.1 slice.116
  172.8 2.4 copy.26
  175.2 34.8 %all-reduce.3.cloned.1.call-done = (bf16[1,768,512]{2,1,0:T(8,128)(2,1)}, bf16[1,768,64]{1,2,0:T(8,128)(2,1)}) async-done(((bf16[1,768,512]{2,1,0:T(8,128)(2,1)}, bf16[1,768,64]{1,2,0:T(8,128)(2,1)}), (bf16[1,768,512]{2,1,0:T(8,128)(2,1)}, bf16[1,768,64]{1,2,0:T(8,128)(2,1)})) %all-reduce.3.cloned.1.call-update) | async-done | bytes 884752 | tf_op jit(solution)/shard_map/psum | solution.py:144
  215.0 48.6 %reduce-scatter.2.cloned.1.call-done = f32[64,2048]{1,0:T(8,128)} async-done(((f32[512,2048]{1,0:T(8,128)}), f32[64,2048]{1,0:T(8,128)}) %reduce-scatter.2.cloned.1.call-update) | async-done | bytes 524304 | tf_op jit(solution)/shard_map/reduce_scatter | solution.py:152
  (123 shorter events, 71.0 us)
Async XLA Ops:
  7.2 28.8 %all-gather.5.cloned.1.call-start = ((), (), s32[]{:S(2)}) async-start(), calls=%async_computation.2 | async-start | bytes 1179648 | tf_op jit(solution)/shard_map/all_gather | solution.py:112
  7.9 53.4 %all-gather.3.cloned.1.call-start = ((), (), s32[]{:S(2)}) async-start(), calls=%async_computation.1 | async-start | bytes 1179648 | tf_op jit(solution)/shard_map/all_gather | solution.py:111
  8.6 201.4 %all-reduce.3.cloned.1.call-start = ((), (), s32[]{:S(2)}) async-start(), calls=%async_computation.4 | async-start | bytes 1769472 | tf_op jit(solution)/shard_map/psum | solution.py:144
  8.7 8.4 %copy-start.10 = (f32[32]{0:T(128)}, f32[32]{0:T(128)S(1)}, u32[]{:S(2)}) copy-start(f32[32]{0:T(128)S(1)} %negate_power_fusion) | copy-start | bytes 388
  15.7 1.1 copy-start
  17.5 0.6 copy-start.2
  17.5 0.7 copy-start.4
  18.2 17.8 %copy-start.8 = (f32[512]{0:T(512)S(1)}, f32[512]{0:T(512)}, u32[]{:S(2)}) copy-start(f32[512]{0:T(512)} %param.13) | copy-start | bytes 6148
  19.8 41.5 %copy-start.6 = (f32[768]{0:T(1024)}, f32[768]{0:T(1024)S(1)}, u32[]{:S(2)}) copy-start(f32[768]{0:T(1024)S(1)} %get-tuple-element.145) | copy-start | bytes 9220
  155.1 4.3 %copy-start.14 = (bf16[512,1024]{1,0:T(8,128)(2,1)S(1)}, bf16[512,1024]{1,0:T(8,128)(2,1)}, u32[]{:S(2)}) copy-start(bf16[512,1024]{1,0:T(8,128)(2,1)} %all-gather.3.cloned.1.call-done) | copy-start | bytes 3145732
  159.4 1.4 copy-start.12
  159.4 1.7 copy-start.13
  161.1 2.2 copy-start.7
  161.1 2.2 copy-start.9
  163.1 100.4 %reduce-scatter.2.cloned.1.call-start = ((), (), s32[]{:S(2)}) async-start(), calls=%async_computation.3 | async-start | bytes 4718592 | tf_op jit(solution)/shard_map/reduce_scatter | solution.py:152
  168.9 2.1 copy-start.3
  168.9 2.1 copy-start.5
  172.8 38.3 %copy-start.11 = (f32[32]{0:T(128)S(1)}, f32[32]{0:T(128)}, u32[]{:S(2)}) copy-start(f32[32]{0:T(128)} %copy-done.10) | copy-start | bytes 388
  210.1 3.6 %copy-start.1 = (bf16[1,768,512]{2,1,0:T(8,128)(2,1)S(1)}, bf16[1,768,512]{2,1,0:T(8,128)(2,1)}, u32[]{:S(2)}) copy-start(bf16[1,768,512]{2,1,0:T(8,128)(2,1)} %get-tuple-element.126) | copy-start | bytes 2359300
Sparse Core Ops, SparseCore 0:
  9.9 26.0 all-gather.4
  37.9 23.3 all-gather.2
  163.2 46.8 all-reduce.2
  213.3 50.2 reduce-scatter.1
where the time goes:
time: 274 us; the launch traced here: 272 us
  waiting for transfers between devices  123 us (45%)
  matrix products  87 us (32%)
  local copies, waits for them, and re-layouts  24.8 us (9%)
  other arithmetic  22.9 us (8%)
  between operations  14.1 us (5%)
    reduce_scatter x1, waiting for transfers between devices, shards(): lax.psum_scatter(product * grad_scale, 'dp', scatter_dimension=0, tiled=T...  48.6 us
    psum x1, waiting for transfers between devices, shards(): lax.psum(comp_part.astype(jnp.bfloat16), 'sp').astype(jnp.float32)  34.8 us
    all_gather x1, waiting for transfers between devices, shards(): lax.all_gather(key_up, 'dp', axis=0, tiled=True)  21.6 us
    dot_general x8, matrix products, head_backward(): jnp.dot(score_grad.T, query_used, preferred_element_type=jnp.float32)  18.9 us
    dot_general x8, matrix products, head_backward(): jnp.dot(score_grad, key_used, preferred_element_type=jnp.float32)  18.1 us
    all_gather x1, waiting for transfers between devices, shards(): lax.all_gather(value_up, 'dp', axis=0, tiled=True)  16.2 us
    dot_general x8, matrix products, head_backward(): jnp.dot(head_grad, head_value.T, preferred_element_type=jnp.float32)  12.8 us
    dot_general x8, matrix products, head_backward(): jnp.dot(query_used, key_used.T, preferred_element_type=jnp.float32)  12.7 us
  transfers between devices with their start and end apart: 4, of which 4 were waited for; matrix products, arithmetic and copies ran while one was open for 11% of the time, Pallas kernels for 0%

commit v1 on v0

--- a/solution.py
+++ b/solution.py
@@ -141,7 +141,9 @@
         batch_count * seq_count, -1
     )
     grad_scale = float(lax.axis_size("dp") * batch_count * seq_count) ** (-0.5)
-    comp_total = lax.psum(comp_part.astype(jnp.bfloat16), "sp").astype(jnp.float32)
+    comp_total = jnp.sum(lax.all_gather(comp_part.astype(jnp.bfloat16), "sp"), axis=0).astype(
+        jnp.float32
+    )
     rot_total = lax.psum(rot_part.astype(jnp.bfloat16), "sp").astype(jnp.float32)
     latent_grad, rope_grad = finish(
         comp_total, rot_total, raw_latent, inverse, kv_gain, cosine, sine_table

time: 274 us -> 322 us (1.18)
  waiting for transfers between devices: 123 us -> 170 us
    all_gather x0 -> x1, waiting for transfers between devices: none -> 63.2 us  [shards(): lax.all_gather(comp_part.astype(jnp.bfloat16), 'sp')]
    psum x1, waiting for transfers between devices: 34.8 us -> 18.8 us  [shards(): lax.psum(rot_part.astype(jnp.bfloat16), 'sp').astype(jnp.float32)]
    unnamed x33 -> x31, local copies, waits for them, and re-layouts: 9.88 us -> 9.88 us
  transfers between devices with their start and end apart: 4 -> 5, of which waited for: 4 -> 5; matrix products, arithmetic and copies ran while one was open for 11% -> 11% of each run, Pallas kernels for 0% -> 0%
where the time goes in v1:
time: 322 us; the launch traced here: 321 us
  waiting for transfers between devices  170 us (53%)
  matrix products  87 us (27%)
  local copies, waits for them, and re-layouts  24.8 us (8%)
  other arithmetic  24.5 us (8%)
  between operations  14.1 us (4%)
    all_gather x1, waiting for transfers between devices, shards(): lax.all_gather(comp_part.astype(jnp.bfloat16), 'sp')  63.2 us
    reduce_scatter x1, waiting for transfers between devices, shards(): lax.psum_scatter(product * grad_scale, 'dp', scatter_dimension=0, tiled=T...  48.5 us
    all_gather x1, waiting for transfers between devices, shards(): lax.all_gather(key_up, 'dp', axis=0, tiled=True)  21.6 us
    dot_general x8, matrix products, head_backward(): jnp.dot(score_grad.T, query_used, preferred_element_type=jnp.float32)  19 us
    psum x1, waiting for transfers between devices, shards(): lax.psum(rot_part.astype(jnp.bfloat16), 'sp').astype(jnp.float32)  18.8 us
    dot_general x8, matrix products, head_backward(): jnp.dot(score_grad, key_used, preferred_element_type=jnp.float32)  18 us
    all_gather x1, waiting for transfers between devices, shards(): lax.all_gather(value_up, 'dp', axis=0, tiled=True)  16.2 us
    dot_general x8, matrix products, head_backward(): jnp.dot(head_grad, head_value.T, preferred_element_type=jnp.float32)  12.8 us
  transfers between devices with their start and end apart: 5, of which 5 were waited for; matrix products, arithmetic and copies ran while one was open for 11% of the time, Pallas kernels for 0%

profile of v1, /device:TPU:0, one launch (start us, length us, event | category | flops | bytes accessed | tf_op | source)
XLA Modules:
  0.0 320.8 jit_solution(13778856997985525466)
XLA Ops:
  10.3 2.6 copy.21
  12.9 2.8 copy.18
  19.8 16.2 %all-gather.7.cloned.1.call-done = bf16[512,1024]{1,0:T(8,128)(2,1)} async-done(((bf16[64,1024]{1,0:T(8,128)(2,1)}), bf16[512,1024]{1,0:T(8,128)(2,1)}) %all-gather.7.cloned.1.call-update) | async-done | bytes 1048592 | tf_op jit(solution)/shard_map/all_gather | solution.py:112
  36.0 2.3 fusion.44
  39.7 21.6 %all-gather.5.cloned.1.call-done = bf16[512,1024]{1,0:T(8,128)(2,1)} async-done(((bf16[64,1024]{1,0:T(8,128)(2,1)}), bf16[512,1024]{1,0:T(8,128)(2,1)}) %all-gather.5.cloned.1.call-update) | async-done | bytes 1048592 | tf_op jit(solution)/shard_map/all_gather | solution.py:111
  61.3 2.3 fusion.43
  64.0 2.3 pad_maximum_fusion
  66.4 88.8 %while.19 = (s32[]{:T(128)}, f32[8,768,192]{1,2,0:T(8,128)}, f32[8,768,192]{1,2,0:T(8,128)}, bf16[8,768,128]{1,2,0:T(8,128)(2,1)}, bf16[8,768,192]{1,2,0:T(8,128...) while((s32[]{:T(128)}, f32[8,768,192]{1,2,0:T(8,128)}, ...), condition=%wide.region_5.6_spmd, body=%wide.region_1.5_spmd.sunk | while | flops 992769792 | bytes 24220780 | solution.py:81
  72.8 2.3 fusion.99
  75.2 2.3 fusion.98
  83.9 2.4 fusion.99
  86.3 2.3 fusion.98
  95.0 2.4 fusion.99
  97.4 2.3 fusion.98
  106.1 2.4 fusion.99
  108.5 2.2 fusion.98
  117.2 2.3 fusion.99
  119.6 2.3 fusion.98
  128.3 2.4 fusion.99
  130.7 2.2 fusion.98
  139.4 2.4 fusion.99
  141.8 2.2 fusion.98
  150.5 2.4 fusion.99
  152.9 2.3 fusion.98
  155.1 2.2 slice_reduce_fusion
  163.4 5.5 %convolution_multiply_fusion = f32[512,2048]{1,0:T(8,128)} fusion(bf16[1,768,1024]{1,2,0:T(8,128)(2,1)} %bitcast.137, bf16[1,768,1024]{1,2,0:T(8,128)(2,1)S(1)} %bitcast.135, bf16[1,768,512]{2,1,0:T(8,128)(2,1)S(1)} %copy-done, f32[512]{0:T(512)S(1)} %copy-done.8, f32[768]{0:T(1024)S(1)} %copy-done.6), kind=kOutput, calls=%fused_computation.36 | convolution fusion | flops 1619525632 | bytes 8131584 | tf_op jit(solution)/shard_map/dot_general | solution.py:151
  169.0 2.1 slice.116
  172.9 2.4 copy.26
  175.3 18.8 %all-reduce.2.cloned.1.call-done = bf16[1,768,64]{1,2,0:T(8,128)(2,1)} async-done(((bf16[1,768,64]{1,2,0:T(8,128)(2,1)}), bf16[1,768,64]{1,2,0:T(8,128)(2,1)}) %all-reduce.2.cloned.1.call-update) | async-done | bytes 98320 | tf_op jit(solution)/shard_map/psum | solution.py:147
  196.1 63.2 %all-gather.9.cloned.1.call-done = bf16[3072,512]{1,0:T(8,128)(2,1)} async-done(((bf16[768,512]{1,0:T(8,128)(2,1)}), bf16[3072,512]{1,0:T(8,128)(2,1)}) %all-gather.9.cloned.1.call-update) | async-done | bytes 3145744 | tf_op jit(solution)/shard_map/all_gather | solution.py:144
  259.3 2.8 reduce.4
  263.8 48.5 %reduce-scatter.2.cloned.1.call-done = f32[64,2048]{1,0:T(8,128)} async-done(((f32[512,2048]{1,0:T(8,128)}), f32[64,2048]{1,0:T(8,128)}) %reduce-scatter.2.cloned.1.call-update) | async-done | bytes 524304 | tf_op jit(solution)/shard_map/reduce_scatter | solution.py:154
  (125 shorter events, 73.8 us)
Async XLA Ops:
  7.2 28.8 %all-gather.7.cloned.1.call-start = ((), (), s32[]{:S(2)}) async-start(), calls=%async_computation.2 | async-start | bytes 1179648 | tf_op jit(solution)/shard_map/all_gather | solution.py:112
  7.9 53.4 %all-gather.5.cloned.1.call-start = ((), (), s32[]{:S(2)}) async-start(), calls=%async_computation.1 | async-start | bytes 1179648 | tf_op jit(solution)/shard_map/all_gather | solution.py:111
  8.6 185.5 %all-reduce.2.cloned.1.call-start = ((), (), s32[]{:S(2)}) async-start(), calls=%async_computation.3 | async-start | bytes 196608 | tf_op jit(solution)/shard_map/psum | solution.py:147
  8.7 8.4 %copy-start.9 = (f32[32]{0:T(128)}, f32[32]{0:T(128)S(1)}, u32[]{:S(2)}) copy-start(f32[32]{0:T(128)S(1)} %negate_power_fusion) | copy-start | bytes 388
  15.7 1.1 copy-start
  17.5 0.6 copy-start.1
  17.5 0.7 copy-start.3
  18.2 17.8 %copy-start.7 = (f32[512]{0:T(512)S(1)}, f32[512]{0:T(512)}, u32[]{:S(2)}) copy-start(f32[512]{0:T(512)} %param.13) | copy-start | bytes 6148
  19.8 41.5 %copy-start.5 = (f32[768]{0:T(1024)}, f32[768]{0:T(1024)S(1)}, u32[]{:S(2)}) copy-start(f32[768]{0:T(1024)S(1)} %get-tuple-element.143) | copy-start | bytes 9220
  155.1 4.4 %copy-start.13 = (bf16[512,1024]{1,0:T(8,128)(2,1)S(1)}, bf16[512,1024]{1,0:T(8,128)(2,1)}, u32[]{:S(2)}) copy-start(bf16[512,1024]{1,0:T(8,128)(2,1)} %all-gather.5.cloned.1.call-done) | copy-start | bytes 3145732
  159.5 99.9 %all-gather.9.cloned.1.call-start = ((), (), s32[]{:S(2)}) async-start(), calls=%async_computation.5 | async-start | bytes 3932160 | tf_op jit(solution)/shard_map/all_gather | solution.py:144
  159.5 1.4 copy-start.11
  159.5 1.7 copy-start.12
  161.2 2.2 copy-start.6
  161.2 2.2 copy-start.8
  163.2 149.2 %reduce-scatter.2.cloned.1.call-start = ((), (), s32[]{:S(2)}) async-start(), calls=%async_computation.4 | async-start | bytes 4718592 | tf_op jit(solution)/shard_map/reduce_scatter | solution.py:154
  169.0 2.1 copy-start.2
  169.0 2.1 copy-start.4
  172.9 22.1 %copy-start.10 = (f32[32]{0:T(128)S(1)}, f32[32]{0:T(128)}, u32[]{:S(2)}) copy-start(f32[32]{0:T(128)} %copy-done.9) | copy-start | bytes 388
Sparse Core Ops, SparseCore 0:
  9.9 26.0 all-gather.6
  37.9 23.3 all-gather.4
  159.6 34.4 all-reduce.1
  196.1 63.1 all-gather.8
  262.5 49.7 reduce-scatter.1
